TPU v7x, 32 devices: a whole 2x2x4 slice. The times are simulated.
32 devices in a mesh: sp: 8 (over z, x), tp: 4 (over y, core).
Axes of the slice: x: 2, y: 2, z: 4, core: 2. Of those that a mesh axis runs over, the one named last changes fastest.
Arguments:
- tokens: bfloat16 [2048, 2048], P('sp', 'tp'), may hold values from -6 to 6
- norm_gain: float32 [2048], replicated, may hold values from 0.1 to 1.9
- query_one: bfloat16 [2048, 512], P('sp', 'tp'), may hold values from -1 to 1
- key_one: bfloat16 [2048, 512], P('sp', 'tp'), may hold values from -1 to 1
- query_two: bfloat16 [2048, 512], P('sp', 'tp'), may hold values from -0.15625 to 0.15625
- key_two: bfloat16 [2048, 512], P('sp', 'tp'), may hold values from -0.15625 to 0.15625
- value_weight: bfloat16 [2048, 1024], P('sp', 'tp'), may hold values from -0.5 to 0.5
- pool_weight: bfloat16 [2048, 1024], P('sp', 'tp'), may hold values from -0.125 to 0.125
- lambda_head: float32 [8], replicated, may hold values from 0.3 to 0.8
- head_gain: float32 [128], replicated, may hold values from 0.1 to 1.9
- group_weight: bfloat16 [8, 128, 128], replicated, may hold values from -0.5 to 0.5
- pool_scale: float32 [1024], replicated, may hold values from 0.1 to 1.9
- out_attn: bfloat16 [1024, 2048], P('tp', 'sp'), may hold values from -0.125 to 0.125
- out_pool: bfloat16 [1024, 2048], P('tp', 'sp'), may hold values from -0.125 to 0.125
Outputs:
- mixed: bfloat16 [2048, 2048], P(('sp', 'tp'))
All inputs are finite; a program needn't handle non-finite values.
Results may differ from a plain program's by a relative error of at most 0.013.
Values may be sent and summed in bfloat16 or wider, within the bound.
A program may use at most 128 MiB of HBM per device.

v0:
```python
import math

import jax
import jax.numpy as jnp
from jax import lax
from jax.sharding import PartitionSpec as P

HEAD_DIM = 64
VALUE_DIM = 128
GROUP_DIM = 128


rope_base = 500000.0
head_scale = 0.8
norm_floor = 1e-06
head_floor = 0.001
masked_score = -1e30
pool_reach = 15
key_block = 1024


def from_behind(x, axis, by):
    peers = lax.axis_size(axis)
    pairs = [(i, i + by) for i in range(peers) if 0 <= i + by < peers]
    return lax.ppermute(x, axis, pairs)


def rotate(values_in, positions):
    half_dim = values_in.shape[-1] // 2
    inverse = rope_base ** (-(jnp.arange(half_dim, dtype=jnp.float32) * 2.0 / values_in.shape[-1]))
    angles = positions.astype(jnp.float32)[:, None] * inverse[None, :]
    cosine = jnp.cos(angles)[:, None, :]
    sine_part = jnp.sin(angles)[:, None, :]
    first_half = values_in[..., :half_dim]
    second_half = values_in[..., half_dim:]
    return jnp.concatenate(
        [
            first_half * cosine - second_half * sine_part,
            second_half * cosine + first_half * sine_part,
        ],
        axis=-1,
    )


def body(
    tokens,
    norm_gain,
    query_one,
    key_one,
    query_two,
    key_two,
    value_weight,
    pool_weight,
    lambda_head,
    head_gain,
    group_weight,
    pool_scale,
    out_attn,
    out_pool,
):
    tok_rows = tokens.shape[0]
    local_heads = query_one.shape[1] // HEAD_DIM
    local_groups = pool_weight.shape[1] // GROUP_DIM
    tp_index = lax.axis_index("tp")
    positions = lax.axis_index("sp") * tok_rows + jnp.arange(tok_rows, dtype=jnp.int32)
    score_scale = HEAD_DIM ** (-0.5)
    gathered = lax.all_gather(tokens, "tp", axis=1, tiled=True)
    float_rows = gathered.astype(jnp.float32)
    normed = (
        float_rows
        * lax.rsqrt(jnp.mean(float_rows * float_rows, axis=-1, keepdims=True) + norm_floor)
        * norm_gain
    ).astype(jnp.bfloat16)

    def contract(shard_part):
        return jnp.dot(normed, shard_part, preferred_element_type=jnp.float32)

    pieces = (
        lax.all_gather(query_one, "sp", axis=0, tiled=True),
        lax.all_gather(key_one, "sp", axis=0, tiled=True),
        lax.all_gather(query_two, "sp", axis=0, tiled=True),
        lax.all_gather(key_two, "sp", axis=0, tiled=True),
        lax.all_gather(value_weight, "sp", axis=0, tiled=True),
    )
    projected = tuple((contract(shard_part) for shard_part in pieces))
    pool_proj = contract(lax.all_gather(pool_weight, "sp", axis=0, tiled=True))

    def turned(flat_part):
        return rotate(flat_part.reshape(tok_rows, local_heads, HEAD_DIM), positions).astype(
            jnp.bfloat16
        )

    query_a = turned(projected[0])
    key_a = turned(projected[1]).reshape(tok_rows, local_heads * HEAD_DIM)
    query_b = turned(projected[2])
    key_b = turned(projected[3]).reshape(tok_rows, local_heads * HEAD_DIM)
    value_rows = projected[4].astype(jnp.bfloat16)
    queries = (query_a, query_b)
    initial = (
        jnp.full((2, tok_rows, local_heads), masked_score, jnp.float32),
        jnp.zeros((2, tok_rows, local_heads), jnp.float32),
        jnp.zeros((2, tok_rows, local_heads, VALUE_DIM), jnp.float32),
    )
    pieces = (
        lax.all_gather(key_a, "sp", axis=0, tiled=True),
        lax.all_gather(key_b, "sp", axis=0, tiled=True),
        lax.all_gather(value_rows, "sp", axis=0, tiled=True),
    )
    key_rows = pieces[0].shape[0]
    key_span = math.gcd(key_rows, key_block)
    count_blocks = key_rows // key_span
    stacked = tuple((member.reshape(count_blocks, key_span, local_heads, -1) for member in pieces))

    def step_block(carried, inputs):
        maxima, totals, accums = carried
        block_a, block_b, block_v, block_id = inputs
        key_pos = block_id * key_span + jnp.arange(key_span, dtype=jnp.int32)
        visible = (key_pos[None, :] <= positions[:, None])[:, None, :]
        new_maxima, new_totals, new_accums = ([], [], [])
        for map_index, key_part in enumerate((block_a, block_b)):
            scores = (
                jnp.einsum(
                    "qhd,khd->qhk", queries[map_index], key_part, preferred_element_type=jnp.float32
                )
                * score_scale
            )
            scores = jnp.where(visible, scores, masked_score)
            top_now = jnp.maximum(maxima[map_index], jnp.max(scores, axis=-1))
            factor = jnp.exp(maxima[map_index] - top_now)
            weights = jnp.where(visible, jnp.exp(scores - top_now[..., None]), 0.0)
            new_maxima.append(top_now)
            new_totals.append(totals[map_index] * factor + jnp.sum(weights, axis=-1))
            product = jnp.einsum(
                "qhk,khd->qhd",
                weights.astype(jnp.bfloat16),
                block_v,
                preferred_element_type=jnp.float32,
            )
            new_accums.append(accums[map_index] * factor[..., None] + product)
        return ((jnp.stack(new_maxima), jnp.stack(new_totals), jnp.stack(new_accums)), None)

    result_state, _ = lax.scan(
        step_block,
        initial,
        (stacked[0], stacked[1], stacked[2], jnp.arange(count_blocks, dtype=jnp.int32)),
    )
    maxima, totals, accums = result_state
    map_means = accums / totals[..., None]
    lambda_local = lax.dynamic_slice_in_dim(lambda_head, tp_index * local_heads, local_heads, 0)
    differed = map_means[0] - lambda_local[None, :, None] * map_means[1]
    scaled = (
        differed
        * lax.rsqrt(jnp.mean(differed * differed, axis=-1, keepdims=True) + head_floor)
        * head_gain
        * head_scale
    )
    attn_out = scaled.reshape(tok_rows, local_heads * VALUE_DIM).astype(jnp.bfloat16)
    pool_rows = pool_proj.astype(jnp.bfloat16)
    prior_rows = from_behind(pool_rows[tok_rows - pool_reach :], "sp", 1)
    extended = jnp.concatenate([prior_rows, pool_rows], axis=0).astype(jnp.float32)
    group_ids = tp_index * local_groups + jnp.arange(local_groups, dtype=jnp.int32)
    windows = jnp.left_shift(2, group_ids % 4)
    channel_windows = (windows[:, None] + jnp.zeros((1, GROUP_DIM), jnp.int32)).reshape(-1)
    window_sum = jnp.zeros((tok_rows, local_groups * GROUP_DIM), jnp.float32)
    for lag_steps in range(pool_reach + 1):
        keep_mask = (lag_steps < channel_windows).astype(jnp.float32)
        window_sum = (
            window_sum
            + extended[pool_reach - lag_steps : pool_reach - lag_steps + tok_rows]
            * keep_mask[None, :]
        )
    counts = jnp.minimum(positions[:, None] + 1, channel_windows[None, :]).astype(jnp.float32)
    window_mean = window_sum / counts - pool_rows.astype(jnp.float32)
    local_mixing = lax.dynamic_slice_in_dim(group_weight, tp_index * local_groups, local_groups, 0)
    grouped = jnp.einsum(
        "tgc,gcd->tgd",
        window_mean.astype(jnp.bfloat16).reshape(tok_rows, local_groups, GROUP_DIM),
        local_mixing,
        preferred_element_type=jnp.float32,
    )
    scale_local = lax.dynamic_slice_in_dim(
        pool_scale, tp_index * local_groups * GROUP_DIM, local_groups * GROUP_DIM, 0
    )
    pooled = (grouped.reshape(tok_rows, local_groups * GROUP_DIM) * scale_local).astype(
        jnp.bfloat16
    )
    attn_cols, pool_cols = (
        lax.all_gather(out_attn, "sp", axis=1, tiled=True),
        lax.all_gather(out_pool, "sp", axis=1, tiled=True),
    )
    return lax.psum_scatter(
        (
            jnp.dot(attn_out, attn_cols, preferred_element_type=jnp.float32)
            + jnp.dot(pooled, pool_cols, preferred_element_type=jnp.float32)
        ).astype(jnp.bfloat16),
        "tp",
        scatter_dimension=0,
        tiled=True,
    )


def solution(mesh):
    in_specs = (
        P("sp", "tp"),
        P(),
        P("sp", "tp"),
        P("sp", "tp"),
        P("sp", "tp"),
        P("sp", "tp"),
        P("sp", "tp"),
        P("sp", "tp"),
        P(),
        P(),
        P(),
        P(),
        P("tp", "sp"),
        P("tp", "sp"),
    )
    out_specs = P(("sp", "tp"), None)
    return jax.shard_map(body, mesh=mesh, in_specs=in_specs, out_specs=out_specs, check_vma=False)
```

profile of v0, /device:TPU:26, one launch (start us, length us, event | category | flops | bytes accessed | tf_op | source)
XLA Modules:
  0.0 333.9 jit_solution(8059476277659263844)
XLA Ops:
  6.5 0.7 all-gather.7.cloned.1.call-update
  7.3 0.7 all-gather.9.cloned.1.call-update
  8.1 0.7 all-gather.15.cloned.1.call-update
  8.8 17.8 %all-gather.7.cloned.1.call-done = bf16[256,2048]{1,0:T(8,128)(2,1)} async-done(((bf16[256,512]{1,0:T(8,128)(2,1)}), bf16[256,2048]{1,0:T(8,128)(2,1)}) %all-gather.7.cloned.1.call-update) | async-done | bytes 1048592 | tf_op jit(solution)/shard_map/all_gather | solution.py:67
  26.6 1.5 fusion.41
  28.1 1.6 fusion.43
  29.7 37.1 %all-gather.9.cloned.1.call-done = bf16[2048,256]{1,0:T(8,128)(2,1)} async-done(((bf16[256,256]{1,0:T(8,128)(2,1)}), bf16[2048,256]{1,0:T(8,128)(2,1)}) %all-gather.9.cloned.1.call-update) | async-done | bytes 1048592 | tf_op jit(solution)/shard_map/all_gather | solution.py:83
  66.8 2.3 convolution_convert_fusion.1
  71.6 31.9 %all_gather.37 = bf16[2048,128]{1,0:T(8,128)(2,1)S(1)} all-gather(bf16[256,128]{1,0:T(8,128)(2,1)S(1)} %copy-done.4), channel_id=1, replica_groups=mesh['sp'=8,'tp'=4] {'sp'}, dimensions={0}, use_global_device_ids=true | all-gather | bytes 589824 | tf_op jit(solution)/shard_map/all_gather | solution.py:80
  103.6 31.8 %all_gather.39 = bf16[2048,128]{1,0:T(8,128)(2,1)S(1)} all-gather(bf16[256,128]{1,0:T(8,128)(2,1)S(1)} %copy-done.5), channel_id=1, replica_groups=mesh['sp'=8,'tp'=4] {'sp'}, dimensions={0}, use_global_device_ids=true | all-gather | bytes 589824 | tf_op jit(solution)/shard_map/all_gather | solution.py:79
  135.4 32.3 %all_gather.40 = bf16[2048,128]{1,0:T(8,128)(2,1)S(1)} all-gather(bf16[256,128]{1,0:T(8,128)(2,1)S(1)} %copy-done.6), channel_id=1, replica_groups=mesh['sp'=8,'tp'=4] {'sp'}, dimensions={0}, use_global_device_ids=true | all-gather | bytes 589824 | tf_op jit(solution)/shard_map/all_gather | solution.py:82
  167.7 32.3 %all_gather.42 = bf16[2048,128]{1,0:T(8,128)(2,1)S(1)} all-gather(bf16[256,128]{1,0:T(8,128)(2,1)S(1)} %copy-done.7), channel_id=1, replica_groups=mesh['sp'=8,'tp'=4] {'sp'}, dimensions={0}, use_global_device_ids=true | all-gather | bytes 589824 | tf_op jit(solution)/shard_map/all_gather | solution.py:81
  200.2 0.7 dynamic_slice.24
  201.0 0.8 dynamic_slice.26
  203.8 31.9 %all_gather.41 = bf16[2048,128]{0,1:T(8,128)(2,1)S(1)} all-gather(bf16[256,128]{0,1:T(8,128)(2,1)S(1)} %bitcast.251), channel_id=1, replica_groups=mesh['sp'=8,'tp'=4] {'sp'}, dimensions={0}, use_global_device_ids=true | all-gather | bytes 589824 | tf_op jit(solution)/shard_map/all_gather | solution.py:106
  235.7 31.2 %all_gather.38 = bf16[2048,128]{0,1:T(8,128)(2,1)S(1)} all-gather(bf16[256,128]{0,1:T(8,128)(2,1)S(1)} %bitcast.252), channel_id=1, replica_groups=mesh['sp'=8,'tp'=4] {'sp'}, dimensions={0}, use_global_device_ids=true | all-gather | bytes 589824 | tf_op jit(solution)/shard_map/all_gather | solution.py:105
  266.9 1.7 convolution_convert_fusion
  268.6 1.5 collective-permute-start
  270.5 0.9 copy.23
  271.9 2.2 collective-permute-done
  274.2 0.7 fusion.70
  275.1 1.3 reshape.313
  276.5 18.7 %while.15 = (s32[]{:T(128)}, f32[2,256,2]{1,2,0:T(2,128)S(1)}, f32[2,256,2]{1,2,0:T(2,128)S(1)}, f32[2,256,2,128]{1,3,2,0:T(8,128)S(1)}, s32[2]{0:T(128)S(1)}, /...) while((s32[]{:T(128)}, f32[2,256,2]{1,2,0:T(2,128)S(1)}, ...), condition=%wide.region_6.7_spmd.clone, body=%wide.region_1.6_spmd.clone.sunk | while | flops 416947456 | bytes 34822424 | solution.py:142
  278.1 1.8 fusion.141
  280.8 2.4 fusion.147
  283.2 1.0 fusion.143
  287.4 1.8 fusion.141
  290.1 2.4 fusion.147
  292.5 1.0 fusion.143
  295.6 1.7 fusion.101
  297.3 2.7 fusion.40
  300.1 27.0 %reduce-scatter.2.cloned.1.call-done = bf16[64,2048]{1,0:T(8,128)(2,1)} async-done(((bf16[256,2048]{1,0:T(8,128)(2,1)}), bf16[64,2048]{1,0:T(8,128)(2,1)}) %reduce-scatter.2.cloned.1.call-update) | async-done | bytes 262160 | tf_op jit(solution)/shard_map/reduce_scatter | solution.py:191
  (105 shorter events, 13.1 us)
Async XLA Ops:
  6.5 267.6 %copy-start = (bf16[8,128,128]{2,1,0:T(8,128)(2,1)S(1)}, bf16[8,128,128]{2,1,0:T(8,128)(2,1)}, u32[]{:S(2)}) copy-start(bf16[8,128,128]{2,1,0:T(8,128)(2,1)} %param.26) | copy-start | bytes 786436
  6.5 20.0 %all-gather.7.cloned.1.call-start = ((), (), s32[]{:S(2)}) async-start(), calls=%async_computation.1 | async-start | bytes 1310720 | tf_op jit(solution)/shard_map/all_gather | solution.py:67
  7.3 59.6 %all-gather.9.cloned.1.call-start = ((), (), s32[]{:S(2)}) async-start(), calls=%async_computation.2 | async-start | bytes 1179648 | tf_op jit(solution)/shard_map/all_gather | solution.py:83
  8.0 258.9 %all-gather.15.cloned.1.call-start = ((), (), s32[]{:S(2)}) async-start(), calls=%async_computation.5 | async-start | bytes 1179648 | tf_op jit(solution)/shard_map/all_gather | solution.py:86
  8.7 266.3 %all-gather.11.cloned.1.call-start = ((), (), s32[]{:S(2)}) async-start(), calls=%async_computation.3 | async-start | bytes 1179648 | tf_op jit(solution)/shard_map/all_gather | solution.py:107
  28.1 43.5 %copy-start.4 = (bf16[256,128]{1,0:T(8,128)(2,1)S(1)}, bf16[256,128]{1,0:T(8,128)(2,1)}, u32[]{:S(2)}) copy-start(bf16[256,128]{1,0:T(8,128)(2,1)} %param.19) | copy-start | bytes 196612
  29.7 73.9 %copy-start.5 = (bf16[256,128]{1,0:T(8,128)(2,1)S(1)}, bf16[256,128]{1,0:T(8,128)(2,1)}, u32[]{:S(2)}) copy-start(bf16[256,128]{1,0:T(8,128)(2,1)} %param.18) | copy-start | bytes 196612
  29.7 105.7 %copy-start.6 = (bf16[256,128]{1,0:T(8,128)(2,1)S(1)}, bf16[256,128]{1,0:T(8,128)(2,1)}, u32[]{:S(2)}) copy-start(bf16[256,128]{1,0:T(8,128)(2,1)} %param.21) | copy-start | bytes 196612
  29.7 138.0 %copy-start.7 = (bf16[256,128]{1,0:T(8,128)(2,1)S(1)}, bf16[256,128]{1,0:T(8,128)(2,1)}, u32[]{:S(2)}) copy-start(bf16[256,128]{1,0:T(8,128)(2,1)} %param.20) | copy-start | bytes 196612
  29.7 171.2 %copy-start.8 = (f32[128]{0:T(128)S(1)}, f32[128]{0:T(128)}, u32[]{:S(2)}) copy-start(f32[128]{0:T(128)} %param.25) | copy-start | bytes 1540
  69.2 226.4 %all-gather.13.cloned.1.call-start = ((), (), s32[]{:S(2)}) async-start(), calls=%async_computation.4 | async-start | bytes 1179648 | tf_op jit(solution)/shard_map/all_gather | solution.py:188
  69.7 227.6 %all-gather.17.cloned.1.call-start = ((), (), s32[]{:S(2)}) async-start(), calls=%async_computation.6 | async-start | bytes 1179648 | tf_op jit(solution)/shard_map/all_gather | solution.py:189
  70.3 256.7 %reduce-scatter.2.cloned.1.call-start = ((), (), s32[]{:S(2)}) async-start(), calls=%async_computation.7 | async-start | bytes 1310720 | tf_op jit(solution)/shard_map/reduce_scatter | solution.py:191
  268.6 5.5 %collective-permute-start = (bf16[15,256]{1,0:T(8,128)(2,1)S(1)}, bf16[15,256]{1,0:T(8,128)(2,1)S(1)}, u32[]{:S(2)}, u32[]{:S(2)}) collective-permute-start(bf16[15,256]{1,0:T(8,128)(2,1)S(1)} %slice.144), channel_id=1, source_target_pairs={{0,4},{4,8},{8,12},{12,16},{16,20},{20,24},{24,28},{1,5},{5,9},{9,... | collective-permute-start | bytes 23048 | tf_op jit(solution)/shard_map/ppermute | solution.py:25
  270.1 4.1 %copy-start.10 = (s32[256]{0:T(256)S(1)}, s32[256]{0:T(256)}, u32[]{:S(2)}) copy-start(s32[256]{0:T(256)} %broadcast_bitcast_fusion.1) | copy-start | bytes 3076
  270.1 4.1 %copy-start.11 = (s32[256]{0:T(256)S(1)}, s32[256]{0:T(256)}, u32[]{:S(2)}) copy-start(s32[256]{0:T(256)} %fusion.91) | copy-start | bytes 3076
  276.5 3.4 %copy-start.2 = (bf16[2,1024,2,64]{1,3,2,0:T(8,128)(2,1)}, bf16[2,1024,2,64]{1,3,2,0:T(8,128)(2,1)S(1)}, u32[]{:S(2)}) copy-start(bf16[2,1024,2,64]{1,3,2,0:T(8,128)(2,1)S(1)} %get-tuple-element.317) | copy-start | bytes 1572868 | tf_op jit(solution)/shard_map/while
  280.8 2.4 copy-start.1
  280.8 2.4 copy-start.9
  284.8 1.0 copy-start.3
  285.9 3.4 %copy-start.2 = (bf16[2,1024,2,64]{1,3,2,0:T(8,128)(2,1)}, bf16[2,1024,2,64]{1,3,2,0:T(8,128)(2,1)S(1)}, u32[]{:S(2)}) copy-start(bf16[2,1024,2,64]{1,3,2,0:T(8,128)(2,1)S(1)} %get-tuple-element.317) | copy-start | bytes 1572868 | tf_op jit(solution)/shard_map/while
  290.1 2.4 copy-start.1
  290.1 2.4 copy-start.9
  294.2 1.0 copy-start.3
Sparse Core Ops, SparseCore 0:
  8.9 17.6 all-gather.6
  28.7 38.0 all-gather.8
  68.9 41.0 all-gather.14
  112.0 42.2 all-gather.10
  156.2 42.2 all-gather.12
  200.3 40.8 all-gather.16
  300.2 26.8 reduce-scatter.1
where the time goes:
time: 336 us; the launch traced here: 334 us
  blocking collectives  191 us (57%)
  waiting for transfers between devices  87.3 us (26%)
  matrix products  22.7 us (7%)
  between operations  13.8 us (4%)
  local copies, waits for them, and re-layouts  9.14 us (3%)
  other arithmetic  6.18 us (2%)
    all_gather x1, waiting for transfers between devices, body(): lax.all_gather(value_weight, 'sp', axis=0, tiled=True)  37.1 us
    all_gather x1, blocking collectives, body(): lax.all_gather(query_two, 'sp', axis=0, tiled=True)  32.3 us
    all_gather x1, blocking collectives, body(): lax.all_gather(key_two, 'sp', axis=0, tiled=True)  32.3 us
    all_gather x1, blocking collectives, body(): lax.all_gather(key_b, 'sp', axis=0, tiled=True)  31.9 us
    all_gather x1, blocking collectives, body(): lax.all_gather(key_one, 'sp', axis=0, tiled=True)  31.9 us
    all_gather x1, blocking collectives, body(): lax.all_gather(query_one, 'sp', axis=0, tiled=True)  31.8 us
    all_gather x1, blocking collectives, body(): lax.all_gather(key_a, 'sp', axis=0, tiled=True)  31.2 us
    reduce_scatter x1, waiting for transfers between devices, body(): lax.psum_scatter((jnp.dot(attn_out, attn_cols, preferred_element_type=jnp...  27 us
  transfers between devices with their start and end apart: 8, of which 4 were waited for; matrix products, arithmetic and copies ran while one was open for 10% of the time, Pallas kernels for 0%

commit v1 on v0

v1 whole, which is shorter than its diff:
```python
import functools

import jax
import jax.numpy as jnp
from jax import lax
from jax.experimental import pallas as pl
from jax.experimental.pallas import tpu as pltpu
from jax.sharding import PartitionSpec as P

HEAD_DIM = 64
VALUE_DIM = 128
GROUP_DIM = 128
ROPE_BASE = 500000.0
HEAD_SCALE = 0.8
NORM_FLOOR = 1e-06
HEAD_FLOOR = 0.001
MASKED = -1e30
TAIL = 16
HALVES = 2
MESH = pl.DeviceIdType.MESH
BF16 = jnp.bfloat16
F32 = jnp.float32


def flip(index, bit):
    return index + bit * (1 - 2 * ((index // bit) % 2))


def kernel(
    sizes,
    tok_ref,
    gain_ref,
    wp_ref,
    op_ref,
    cos_ref,
    sin_ref,
    lam_ref,
    hg_ref,
    gw_ref,
    ps_ref,
    out_ref,
    tokbuf,
    nrm,
    w_all,
    o_all,
    kv,
    q_st,
    m_st,
    l_st,
    acc_st,
    pool,
    tail,
    prior,
    cat,
    part,
    sbuf,
    rbuf,
    tok_send,
    tok_recv,
    w_up,
    w_dn,
    w_recv,
    wx_send,
    o_up,
    o_dn,
    o_recv,
    ox_send,
    kv_send,
    kv_recv,
    pp_send,
    pp_recv,
    rs_send,
    rs_recv,
):
    G, R, TP = sizes
    s = lax.axis_index("sp")
    t = lax.axis_index("tp")
    r = s // G
    g = s % G
    head = t * G + g
    other = s + 1 - 2 * g
    chunk, feats = tok_ref.shape
    rows = G * chunk
    has_up = r + 1 < R
    has_dn = r > 0

    t_bits = []
    bit = 1
    while bit < TP:
        t_bits.append(("t", bit))
        bit *= 2
    x_dim = ("g", 1)
    members = G * TP

    def member(mask):
        gg, tt = g, t
        for kind, b in mask:
            if kind == "g":
                gg = flip(gg, b)
            else:
                tt = flip(tt, b)
        return gg, tt

    def device(mask):
        gg, tt = member(mask)
        return (r * G + gg, tt)

    barrier = pltpu.get_barrier_semaphore()
    for dim in [x_dim] + t_bits:
        pl.semaphore_signal(barrier, inc=1, device_id=device([dim]), device_id_type=MESH)

    @pl.when(has_up)
    def _():
        pl.semaphore_signal(barrier, inc=1, device_id=(s + G, t), device_id_type=MESH)

    @pl.when(has_dn)
    def _():
        pl.semaphore_signal(barrier, inc=1, device_id=(s - G, t), device_id_type=MESH)

    count = 1 + len(t_bits) + jnp.where(has_up, 1, 0) + jnp.where(has_dn, 1, 0)
    pl.semaphore_wait(barrier, count)

    def rdma(src, dst, ss, rs, dev):
        return pltpu.make_async_remote_copy(
            src_ref=src, dst_ref=dst, send_sem=ss, recv_sem=rs, device_id=dev, device_id_type=MESH
        )

    def up_copy(src, buf, k, up, recv):
        return rdma(src, buf.at[k], up.at[k], recv.at[k], (s + G, t))

    def dn_copy(src, buf, k, dn, recv):
        return rdma(src, buf.at[k], dn.at[k], recv.at[k], (s - G, t))

    def send_both(src, buf, k, up, dn, recv):
        @pl.when(has_up)
        def _():
            up_copy(src, buf, k, up, recv).start()

        @pl.when(has_dn)
        def _():
            dn_copy(src, buf, k, dn, recv).start()

    def cross_copy(inp, buf, xs, recv):
        return rdma(inp.at[1 - g], buf.at[s], xs, recv.at[s], (other, t))

    def wait_slot(buf, k, up, recv):
        up_copy(buf.at[k], buf, k, up, recv).wait_recv()

    def line_step(j, buf, up, dn, recv):
        for gg in (g, 1 - g):
            @pl.when(r - 1 - j >= 0)
            def _():
                k = (r - 1 - j) * G + gg
                wait_slot(buf, k, up, recv)

                @pl.when(has_up)
                def _():
                    up_copy(buf.at[k], buf, k, up, recv).start()

            @pl.when(r + 1 + j < R)
            def _():
                k = (r + 1 + j) * G + gg
                wait_slot(buf, k, up, recv)

                @pl.when(has_dn)
                def _():
                    dn_copy(buf.at[k], buf, k, dn, recv).start()

    def drain(buf, up, dn, recv):
        @pl.when(has_up)
        def _():
            @pl.loop(0, (r + 1) * G)
            def _(k):
                up_copy(buf.at[k], buf, k, up, recv).wait_send()

        @pl.when(has_dn)
        def _():
            @pl.loop(r * G, R * G)
            def _(k):
                dn_copy(buf.at[k], buf, k, dn, recv).wait_send()

    tok_dims = t_bits[1:] + [x_dim] + t_bits[:1]
    tok_stages = []
    held = [[]]
    slot = 0
    for dim in tok_dims:
        stage = []
        for mask in held:
            gg, tt = member(mask)
            src = tok_ref if not mask else tokbuf.at[gg, tt]
            stage.append((mask, src, slot))
            slot += 1
        tok_stages.append((dim, stage))
        held = held + [mask + [dim] for mask in held]

    def tok_copy(dim, mask, src, index):
        gg, tt = member(mask)
        return rdma(src, tokbuf.at[gg, tt], tok_send.at[index], tok_recv.at[index], device([dim]))

    def tok_start(i):
        dim, stage = tok_stages[i]
        for mask, src, index in stage:
            tok_copy(dim, mask, src, index).start()

    def tok_wait(i):
        dim, stage = tok_stages[i]
        for mask, src, index in stage:
            gg, tt = member(mask + [dim])
            rdma(
                tokbuf.at[gg, tt], tokbuf.at[gg, tt], tok_send.at[index], tok_recv.at[index],
                device([dim]),
            ).wait_recv()

    send_both(wp_ref.at[g], w_all, s, w_up, w_dn, w_recv)
    cross_copy(wp_ref, w_all, wx_send, w_recv).start()
    tok_start(0)
    w_all[s] = wp_ref[g]
    o_all[s] = op_ref[g]
    tokbuf[g, t] = tok_ref[...]
    wait_slot(w_all, other, w_up, w_recv)
    send_both(w_all.at[other], w_all, other, w_up, w_dn, w_recv)
    stage_count = len(tok_stages)
    tok_wait(0)
    tok_start(1)
    cross_copy(op_ref, o_all, ox_send, o_recv).start()
    line_step(0, w_all, w_up, w_dn, w_recv)
    for i in range(1, stage_count):
        tok_wait(i)
        if i + 1 < stage_count:
            tok_start(i + 1)
            if i < R - 1:
                line_step(i, w_all, w_up, w_dn, w_recv)
    done_steps = min(stage_count - 1, R - 1)

    gain = gain_ref[...]
    tile = chunk // 2

    @pl.loop(0, G * 2)
    def _(b):
        gi = b // 2
        off = pl.multiple_of((b % 2) * tile, tile)
        dst = pl.multiple_of(b * tile, tile)
        total = jnp.zeros((tile, 1), F32)
        for i in range(TP):
            x = tokbuf[gi, i, pl.ds(off, tile), :].astype(F32)
            total = total + jnp.sum(x * x, axis=-1, keepdims=True)
        inv = lax.rsqrt(total / (TP * feats) + NORM_FLOOR)
        for i in range(TP):
            x = tokbuf[gi, i, pl.ds(off, tile), :].astype(F32)
            nrm[pl.ds(dst, tile), i * feats : (i + 1) * feats] = (
                x * inv * gain[:, i * feats : (i + 1) * feats]
            ).astype(BF16)

    if done_steps < R - 1:
        @pl.loop(done_steps, R - 1)
        def _(j):
            line_step(j, w_all, w_up, w_dn, w_recv)

    send_both(op_ref.at[g], o_all, s, o_up, o_dn, o_recv)
    wait_slot(o_all, other, o_up, o_recv)
    send_both(o_all.at[other], o_all, other, o_up, o_dn, o_recv)

    width = wp_ref.shape[2]
    ptile = chunk

    def rope(x, cosine, sine):
        lane = lax.broadcasted_iota(jnp.int32, x.shape, 1)
        near = jnp.where(
            lane % HEAD_DIM < HEAD_DIM // 2,
            pltpu.roll(x, x.shape[1] - HEAD_DIM // 2, 1),
            pltpu.roll(x, HEAD_DIM // 2, 1),
        )
        return x * cosine + near * sine

    @pl.loop(0, rows // ptile)
    def _(b):
        at = pl.ds(pl.multiple_of(b * ptile, ptile), ptile)
        weights = w_all[...].reshape(-1, width)
        y = jnp.dot(nrm[at, :], weights, preferred_element_type=F32)
        cosine = cos_ref[at, :]
        sine = sin_ref[at, :]
        kv[r, at, 0:128] = rope(y[:, 128:256], cosine, sine).astype(BF16)
        kv[r, at, 128:256] = y[:, 256:384].astype(BF16)
        p = y[:, 384:512].astype(BF16)
        pool[pl.ds(pl.multiple_of(TAIL + b * ptile, TAIL), ptile), :] = p.astype(F32)
        tail[...] = p[ptile - TAIL :, :]
        q = rope(y[:, 0:128], cosine, sine).astype(BF16) * jnp.array(HEAD_DIM**-0.5, BF16)
        lane = lax.broadcasted_iota(jnp.int32, q.shape, 1)
        zero = jnp.zeros_like(q)
        q_st[0, at, :] = jnp.where(lane < HEAD_DIM, q, zero)
        q_st[1, at, :] = jnp.where(lane >= HEAD_DIM, q, zero)

    def kv_copy(k):
        return rdma(kv.at[k], kv.at[k], kv_send.at[k], kv_recv.at[k], (s + G, t))

    tail_copy = rdma(tail, prior, pp_send, pp_recv, (s + G, t))

    @pl.when(has_up)
    def _():
        kv_copy(r).start()
        tail_copy.start()

    qtile = rows // 2

    def attend(k, diagonal):
        @pl.loop(0, 4)
        def _(b):
            m_index = b // 2
            at = pl.ds(pl.multiple_of((b % 2) * qtile, qtile), qtile)
            q = q_st[m_index, at, :]
            scores = lax.dot_general(
                q, kv[k, :, 0:128], (((1,), (1,)), ((), ())), preferred_element_type=F32
            )
            if diagonal:
                qpos = (b % 2) * qtile + lax.broadcasted_iota(jnp.int32, scores.shape, 0)
                kpos = lax.broadcasted_iota(jnp.int32, scores.shape, 1)
                scores = jnp.where(kpos <= qpos, scores, MASKED)
            top = jnp.max(scores, axis=-1, keepdims=True)
            if not diagonal:
                old = m_st[m_index, at, :]
                top = jnp.maximum(old, top)
                factor = jnp.exp(old - top)
            weights = jnp.exp(scores - top)
            total = jnp.sum(weights, axis=-1, keepdims=True)
            product = jnp.dot(weights.astype(BF16), kv[k, :, 128:256], preferred_element_type=F32)
            if not diagonal:
                total = total + l_st[m_index, at, :] * factor
                product = product + acc_st[m_index, at, :] * factor
            m_st[m_index, at, :] = top
            l_st[m_index, at, :] = total
            acc_st[m_index, at, :] = product

    attend(r, True)

    @pl.loop(0, R - 1)
    def _(j):
        line_step(j, o_all, o_up, o_dn, o_recv)

        @pl.when(j < r)
        def _():
            k = r - 1 - j
            kv_copy(k).wait_recv()

            @pl.when(has_up)
            def _():
                kv_copy(k).start()

            attend(k, False)

    @pl.when(has_dn)
    def _():
        tail_copy.wait_recv()
        pool[0:TAIL, :] = prior[...].astype(F32)

    @pl.when(r == 0)
    def _():
        pool[0:TAIL, :] = jnp.zeros((TAIL, GROUP_DIM), F32)

    ext = pool[...]
    kind = head % 4
    window = jnp.where(kind == 0, 2, jnp.where(kind == 1, 4, jnp.where(kind == 2, 8, 16)))
    run = ext + pltpu.roll(ext, 1, 0)
    chosen = run
    for power, lag in ((1, 2), (2, 4), (3, 8)):
        run = run + pltpu.roll(run, lag, 0)
        chosen = jnp.where(kind == power, run, chosen)
    spot = r * rows + lax.broadcasted_iota(jnp.int32, (rows, GROUP_DIM), 0)
    counts = jnp.minimum(spot + 1, window).astype(F32)
    mean = chosen[TAIL:, :] / counts - ext[TAIL:, :]
    mixedg = jnp.dot(mean.astype(BF16), gw_ref[head], preferred_element_type=F32)
    cat[:, 128:256] = (mixedg * ps_ref[head]).astype(BF16)

    diff = acc_st[0] / l_st[0] - lam_ref[head] * (acc_st[1] / l_st[1])
    inv = lax.rsqrt(jnp.mean(diff * diff, axis=-1, keepdims=True) + HEAD_FLOOR)
    cat[:, 0:128] = (diff * inv * hg_ref[...] * HEAD_SCALE).astype(BF16)

    share = rows // members
    o_rows = o_all.shape[0] * o_all.shape[1]
    half = o_rows // HALVES
    o_slots = o_all.shape[0] // HALVES
    orders = ([t_bits[0], x_dim] + t_bits[1:], t_bits + [x_dim])

    def block(mask):
        gg, tt = member(mask)
        return pl.ds(pl.multiple_of((gg * TP + tt) * share, share), share)

    def combos(dims):
        found = [[]]
        for dim in dims:
            found = found + [mask + [dim] for mask in found]
        return found

    plans = []
    for h in range(HALVES):
        order = orders[h % 2]
        stages = []
        base = 0
        for i, dim in enumerate(order):
            masks = combos(order[i + 1 :])
            stages.append((dim, masks, base))
            base += len(masks)
        plans.append(stages)

    def rs_copy(h, dim, mask, index):
        at = block([dim] + mask)
        return rdma(
            sbuf.at[h, at, :], rbuf.at[h, index], rs_send.at[h, index], rs_recv.at[h, index],
            device([dim]),
        )

    def rs_start(h, i):
        dim, masks, base = plans[h][i]
        for n, mask in enumerate(masks):
            at = block([dim] + mask)
            sbuf[h, at, :] = part[h, at, :].astype(BF16)
        for n, mask in enumerate(masks):
            rs_copy(h, dim, mask, base + n).start()

    def rs_finish(h, i):
        dim, masks, base = plans[h][i]
        for n, mask in enumerate(masks):
            rs_copy(h, dim, mask, base + n).wait_recv()
            at = block(mask)
            part[h, at, :] = part[h, at, :] + rbuf[h, base + n].astype(F32)

    for h in range(HALVES):
        @pl.loop(0, 4)
        def _(b):
            at = pl.ds(pl.multiple_of(b * (rows // 4), rows // 4), rows // 4)
            columns = o_all[h * o_slots : (h + 1) * o_slots].reshape(half, -1)
            part[h, at, :] = lax.dot_general(
                cat[at, :], columns, (((1,), (1,)), ((), ())), preferred_element_type=F32
            )

        rs_start(h, 0)

    levels = len(plans[0])
    for i in range(levels):
        for h in range(HALVES):
            rs_finish(h, i)
            if i + 1 < levels:
                rs_start(h, i + 1)
    mine = block([])
    for h in range(HALVES):
        out_ref[:, h * half : (h + 1) * half] = part[h, mine, :].astype(BF16)

    cross_copy(wp_ref, w_all, wx_send, w_recv).wait_send()
    cross_copy(op_ref, o_all, ox_send, o_recv).wait_send()
    drain(w_all, w_up, w_dn, w_recv)
    drain(o_all, o_up, o_dn, o_recv)
    for dim, stage in tok_stages:
        for mask, src, index in stage:
            tok_copy(dim, mask, src, index).wait_send()

    @pl.when(has_up)
    def _():
        tail_copy.wait_send()

        @pl.loop(0, r + 1)
        def _(k):
            kv_copy(k).wait_send()

    for h in range(HALVES):
        for dim, masks, base in plans[h]:
            for n, mask in enumerate(masks):
                rs_copy(h, dim, mask, base + n).wait_send()


def body(
    sp,
    tp,
    tokens,
    norm_gain,
    query_one,
    key_one,
    query_two,
    key_two,
    value_weight,
    pool_weight,
    lambda_head,
    head_gain,
    group_weight,
    pool_scale,
    out_attn,
    out_pool,
):
    G = query_one.shape[1] // HEAD_DIM
    assert G == 2 and sp % G == 0
    R = sp // G
    chunk, feats = tokens.shape
    rows = G * chunk
    depth = query_one.shape[0]
    cols = out_attn.shape[1]
    heads = lambda_head.shape[0]
    members = G * tp
    share = rows // members

    def heads_first(w):
        return w.reshape(depth, G, -1)

    packed = jnp.concatenate(
        [
            heads_first(w)
            for w in (query_one, query_two, key_one, key_two, value_weight, pool_weight)
        ],
        axis=2,
    ).transpose(1, 0, 2)
    out_packed = jnp.concatenate(
        [out_attn.reshape(G, VALUE_DIM, cols), out_pool.reshape(G, GROUP_DIM, cols)], axis=1
    ).transpose(0, 2, 1)

    line = lax.axis_index("sp") // G
    half_dim = HEAD_DIM // 2
    lane = jnp.arange(2 * HEAD_DIM, dtype=jnp.int32)
    inverse = ROPE_BASE ** (-((lane % half_dim).astype(F32) * 2.0 / HEAD_DIM))
    positions = line * rows + jnp.arange(rows, dtype=jnp.int32)
    angles = positions.astype(F32)[:, None] * inverse[None, :]
    cosine = jnp.cos(angles)
    sine = jnp.where(lane % HEAD_DIM < half_dim, -1.0, 1.0)[None, :] * jnp.sin(angles)

    width = packed.shape[2]
    depth_out = out_packed.shape[2]
    total_cols = sp * cols
    vm = pl.BlockSpec(memory_space=pltpu.VMEM)
    dma = pltpu.SemaphoreType.DMA
    return pl.pallas_call(
        functools.partial(kernel, (G, R, tp)),
        out_shape=jax.ShapeDtypeStruct((share, total_cols), BF16),
        in_specs=[vm] * 6 + [pl.BlockSpec(memory_space=pltpu.SMEM)] + [vm] * 3,
        out_specs=vm,
        scratch_shapes=[
            pltpu.VMEM((G, tp, chunk, feats), BF16),
            pltpu.VMEM((rows, tp * feats), BF16),
            pltpu.VMEM((sp, depth, width), BF16),
            pltpu.VMEM((sp, cols, depth_out), BF16),
            pltpu.VMEM((R, rows, 256), BF16),
            pltpu.VMEM((2, rows, 128), BF16),
            pltpu.VMEM((2, rows, 1), F32),
            pltpu.VMEM((2, rows, 1), F32),
            pltpu.VMEM((2, rows, VALUE_DIM), F32),
            pltpu.VMEM((TAIL + rows, GROUP_DIM), F32),
            pltpu.VMEM((TAIL, GROUP_DIM), BF16),
            pltpu.VMEM((TAIL, GROUP_DIM), BF16),
            pltpu.VMEM((rows, depth_out), BF16),
            pltpu.VMEM((HALVES, rows, total_cols // HALVES), F32),
            pltpu.VMEM((HALVES, rows, total_cols // HALVES), BF16),
            pltpu.VMEM((HALVES, members - 1, share, total_cols // HALVES), BF16),
            dma((members - 1,)),
            dma((members - 1,)),
            dma((sp,)),
            dma((sp,)),
            dma((sp,)),
            dma,
            dma((sp,)),
            dma((sp,)),
            dma((sp,)),
            dma,
            dma((R,)),
            dma((R,)),
            dma,
            dma,
            dma((HALVES, members - 1)),
            dma((HALVES, members - 1)),
        ],
        compiler_params=pltpu.CompilerParams(
            collective_id=0, has_side_effects=True, vmem_limit_bytes=58 * 1024 * 1024
        ),
    )(
        tokens,
        norm_gain.reshape(1, -1),
        packed,
        out_packed,
        cosine,
        sine,
        lambda_head,
        head_gain.reshape(1, -1),
        group_weight,
        pool_scale.reshape(heads, 1, GROUP_DIM),
    )


def solution(mesh):
    in_specs = (
        P("sp", "tp"),
        P(),
        P("sp", "tp"),
        P("sp", "tp"),
        P("sp", "tp"),
        P("sp", "tp"),
        P("sp", "tp"),
        P("sp", "tp"),
        P(),
        P(),
        P(),
        P(),
        P("tp", "sp"),
        P("tp", "sp"),
    )
    return jax.shard_map(
        functools.partial(body, mesh.shape["sp"], mesh.shape["tp"]),
        mesh=mesh,
        in_specs=in_specs,
        out_specs=P(("sp", "tp"), None),
        check_vma=False,
    )
```

time: 336 us -> 106 us (0.32)
  blocking collectives: 191 us -> 0 us
  Pallas kernels: 0 us -> 92.8 us
  waiting for transfers between devices: 87.3 us -> 0 us
  matrix products: 22.7 us -> 0 us
  between operations: 13.8 us -> 0.15 us
  other arithmetic: 6.18 us -> 2.57 us
    all_gather x6 -> x0, blocking collectives: 191 us -> none  [the longest x1 32.3 us: body(): lax.all_gather(query_two, 'sp', axis=0, tiled=True)]
    pallas_call x0 -> x1, Pallas kernels: none -> 92.8 us  [body(): pl.pallas_call(functools.partial(kernel, (G, R, tp)), out_shape=jax.Shape...]
    all_gather x6 -> x0, waiting for transfers between devices: 54.9 us -> none  [the longest x1 37.1 us: body(): lax.all_gather(value_weight, 'sp', axis=0, tiled=True)]
    reduce_scatter x1 -> x0, waiting for transfers between devices: 27 us -> none  [body(): lax.psum_scatter((jnp.dot(attn_out, attn_cols, preferred_element_type=jnp...]
    dot_general x17 -> x0, matrix products: 22.7 us -> none  [the longest x4 6.04 us: step_block(): jnp.einsum('qhk,khd->qhd', weights.astype(jnp.bfloat16), block_v, preferr...]
    unnamed x18 -> x21, local copies, waits for them, and re-layouts: 1.08 us -> 7.59 us
    dynamic_slice x8 -> x0, local copies, waits for them, and re-layouts: 4.41 us -> none  [the longest x6 2.92 us: body(): lax.scan(step_block, initial, (stacked[0], stacked[1], stacked[2], jnp.ar...]
  transfers between devices with their start and end apart: 8 -> 0, of which waited for: 4 -> 0; matrix products, arithmetic and copies ran while one was open for 10% -> 0% of each run, Pallas kernels for 0% -> 0%
where the time goes in v1:
time: 106 us; the launch traced here: 105 us
  Pallas kernels  92.8 us (88%)
  local copies, waits for them, and re-layouts  9.61 us (9%)
  other arithmetic  2.57 us (2%)
    pallas_call x1, Pallas kernels, body(): pl.pallas_call(functools.partial(kernel, (G, R, tp)), out_shape=jax.Shape...  92.8 us
    unnamed x21, local copies, waits for them, and re-layouts  7.59 us

profile of v1, /device:TPU:26, one launch (start us, length us, event | category | flops | bytes accessed | tf_op | source)
XLA Modules:
  0.0 105.1 jit_solution(16824344254995876226)
XLA Ops:
  0.0 0.9 copy.15
  1.0 0.0 copy-start.4
  1.0 0.1 copy.21
  1.1 0.7 copy-done.4
  1.8 0.1 copy.17
  1.9 0.0 copy-start.5
  1.9 0.1 copy.23
  2.1 0.7 copy-done.5
  2.8 0.1 copy.16
  2.9 0.0 copy-start.6
  2.9 0.1 copy.22
  3.0 0.7 copy-done.6
  3.7 0.1 copy.18
  3.8 0.0 copy-start
  3.9 0.1 copy.24
  4.0 0.8 copy-done
  4.7 0.1 copy.19
  4.9 0.0 copy-start.1
  4.9 0.1 copy.25
  5.0 0.8 copy-done.1
  5.8 0.1 copy.20
  5.9 0.1 copy.26
  6.0 0.0 copy-start.2
  6.0 1.1 %concatenate.6 = bf16[256,2,512]{2,0,1:T(8,128)(2,1)} concatenate(bf16[256,2,64]{2,0,1:T(8,128)(2,1)S(1)} %copy.21, bf16[256,2,64]{2,0,1:T(8,128)(2,1)S(1)} %copy.22, bf16[256,2,64]{2,0,1:T(8,128)(2,1)S(1)} %copy.23, bf16[256,2,64]{2,0,1:T(8,128)(2,1)S(1)} %copy.24, bf16[256,2,128]{2,0,1:T(8,128)(2,1)S(1)} %copy.25, bf16[256,2,128]{2,0,1:T(8,128)(2,1)S(1)} %copy.26), dimensions={2} | concatenate | bytes 1048576 | tf_op jit(solution)/shard_map/concatenate | solution.py:501
  7.1 0.0 copy-done.2
  7.1 0.1 copy.27
  7.2 0.8 copy-done.3
  8.0 0.1 copy.28
  8.1 0.7 maximum_bitcast_fusion.op_ref
  8.8 1.8 %fusion = (f32[512,128]{1,0:T(8,128)}, f32[512,128]{1,0:T(8,128)}) fusion(f32[128]{0:T(128)S(1)} %get-tuple-element.7, f32[128]{0:T(128)S(1)} %get-tuple-element.8, f32[512]{0:T(512)S(1)} %add_convert_fusion), kind=kLoop, calls=%fused_computation.2 | loop fusion | flops 131072 | bytes 527360 | tf_op jit(solution)/shard_map/mul | solution.py:519
  10.6 92.8 %shard_map.136 = bf16[64,2048]{1,0:T(8,128)(2,1)} custom-call(bf16[256,512]{1,0:T(8,128)(2,1)} %tok_ref.1, f32[1,2048]{1,0:T(1,128)} %bitcast.23, bf16[2,256,512]{2,1,0:T(8,128)(2,1)} %bitcast.14, bf16[2,256,256]{2,1,0:T(8,128)(2,1)} %maximum_bitcast_fusion.op_ref, f32[512,128]{1,0:T(8,128)} %get-tuple-element.6.cos_ref, ...), custom_call_target="tpu_custom_call" | custom-call | tf_op jit(solution)/shard_map/pallas_call | solution.py:526
  103.4 1.7 %copy.30 = bf16[64,2048]{1,0:T(8,128)(2,1)} copy(bf16[64,2048]{1,0:T(8,128)(2,1)} %shard_map.136) | data formatting | bytes 524288
  (3 shorter events, 0.0 us)
Async XLA Ops:
  1.0 0.8 copy-start.4
  1.9 0.8 copy-start.5
  2.9 0.8 copy-start.6
  3.8 0.9 copy-start
  4.9 0.9 copy-start.1
  6.0 1.1 %copy-start.2 = (bf16[256,256]{1,0:T(8,128)(2,1)S(1)}, bf16[256,256]{1,0:T(8,128)(2,1)}, u32[]{:S(2)}) copy-start(bf16[256,256]{1,0:T(8,128)(2,1)} %param.26) | copy-start | bytes 393220
  7.1 0.9 copy-start.3

commit v2 on v1

--- a/solution.py
+++ b/solution.py
@@ -2,6 +2,7 @@
 
 import jax
 import jax.numpy as jnp
+import numpy as np
 from jax import lax
 from jax.experimental import pallas as pl
 from jax.experimental.pallas import tpu as pltpu
@@ -16,7 +17,7 @@
 HEAD_FLOOR = 0.001
 MASKED = -1e30
 TAIL = 16
-HALVES = 2
+CHUNKS = 4
 MESH = pl.DeviceIdType.MESH
 BF16 = jnp.bfloat16
 F32 = jnp.float32
@@ -30,15 +31,25 @@
     sizes,
     tok_ref,
     gain_ref,
-    wp_ref,
-    op_ref,
-    cos_ref,
-    sin_ref,
+    q1_ref,
+    k1_ref,
+    q2_ref,
+    k2_ref,
+    v_ref,
+    p_ref,
+    oa_ref,
+    ob_ref,
+    freq_ref,
     lam_ref,
     hg_ref,
     gw_ref,
     ps_ref,
     out_ref,
+    wp_ref,
+    op_ref,
+    cos_ref,
+    sin_ref,
+    yacc,
     tokbuf,
     nrm,
     w_all,
@@ -117,6 +128,17 @@
     def _():
         pl.semaphore_signal(barrier, inc=1, device_id=(s - G, t), device_id_type=MESH)
 
+    def pack(gg):
+        a, b = gg * HEAD_DIM, (gg + 1) * HEAD_DIM
+        c, d = gg * VALUE_DIM, (gg + 1) * VALUE_DIM
+        wp_ref[gg, :, 0:128] = jnp.concatenate([q1_ref[:, a:b], q2_ref[:, a:b]], axis=1)
+        wp_ref[gg, :, 128:256] = jnp.concatenate([k1_ref[:, a:b], k2_ref[:, a:b]], axis=1)
+        wp_ref[gg, :, 256:384] = v_ref[:, c:d]
+        wp_ref[gg, :, 384:512] = p_ref[:, c:d]
+
+    for gg in range(G):
+        pack(gg)
+
     count = 1 + len(t_bits) + jnp.where(has_up, 1, 0) + jnp.where(has_dn, 1, 0)
     pl.semaphore_wait(barrier, count)
 
@@ -215,8 +237,24 @@
     cross_copy(wp_ref, w_all, wx_send, w_recv).start()
     tok_start(0)
     w_all[s] = wp_ref[g]
+    tokbuf[g, t] = tok_ref[...]
+    for gg in range(G):
+        c, d = gg * VALUE_DIM, (gg + 1) * VALUE_DIM
+        op_ref[gg, :, 0:128] = oa_ref[c:d, :].T
+        op_ref[gg, :, 128:256] = ob_ref[c:d, :].T
     o_all[s] = op_ref[g]
-    tokbuf[g, t] = tok_ref[...]
+
+    lane128 = lax.broadcasted_iota(jnp.int32, (chunk, 2 * HEAD_DIM), 1)
+    sign = jnp.where(lane128 % HEAD_DIM < HEAD_DIM // 2, -1.0, 1.0)
+
+    @pl.loop(0, G)
+    def _(b):
+        at = pl.ds(pl.multiple_of(b * chunk, chunk), chunk)
+        spots = r * rows + b * chunk + lax.broadcasted_iota(jnp.int32, (chunk, 2 * HEAD_DIM), 0)
+        angles = spots.astype(F32) * freq_ref[...]
+        cos_ref[at, :] = jnp.cos(angles)
+        sin_ref[at, :] = jnp.sin(angles) * sign
+
     wait_slot(w_all, other, w_up, w_recv)
     send_both(w_all.at[other], w_all, other, w_up, w_dn, w_recv)
     stage_count = len(tok_stages)
@@ -232,7 +270,14 @@
                 line_step(i, w_all, w_up, w_dn, w_recv)
     done_steps = min(stage_count - 1, R - 1)
 
+    def start_o():
+        send_both(op_ref.at[g], o_all, s, o_up, o_dn, o_recv)
+        wait_slot(o_all, other, o_up, o_recv)
+        send_both(o_all.at[other], o_all, other, o_up, o_dn, o_recv)
+
     gain = gain_ref[...]
+    width = wp_ref.shape[2]
+    span = nrm.shape[2]
     tile = chunk // 2
 
     @pl.loop(0, G * 2)
@@ -247,21 +292,47 @@
         inv = lax.rsqrt(total / (TP * feats) + NORM_FLOOR)
         for i in range(TP):
             x = tokbuf[gi, i, pl.ds(off, tile), :].astype(F32)
-            nrm[pl.ds(dst, tile), i * feats : (i + 1) * feats] = (
-                x * inv * gain[:, i * feats : (i + 1) * feats]
-            ).astype(BF16)
+            y = (x * inv * gain[:, i * feats : (i + 1) * feats]).astype(BF16)
+            for n in range(feats // span):
+                nrm[i * (feats // span) + n, pl.ds(dst, tile), :] = y[:, n * span : (n + 1) * span]
+
+    ptile = chunk
+
+    def project(line, first):
+        @pl.loop(0, rows // ptile)
+        def _(b):
+            at = pl.ds(pl.multiple_of(b * ptile, ptile), ptile)
+            weights = w_all[pl.ds(line * G, G)].reshape(span, width)
+            y = jnp.dot(nrm[line, at, :], weights, preferred_element_type=F32)
+            yacc[at, :] = y if first else yacc[at, :] + y
+
+    def project_step(j):
+        @pl.when(r - 1 - j >= 0)
+        def _():
+            project(r - 1 - j, False)
+
+        @pl.when(r + 1 + j < R)
+        def _():
+            project(r + 1 + j, False)
+
+    project(r, True)
+
+    @pl.loop(0, done_steps)
+    def _(j):
+        project_step(j)
 
     if done_steps < R - 1:
         @pl.loop(done_steps, R - 1)
         def _(j):
             line_step(j, w_all, w_up, w_dn, w_recv)
 
-    send_both(op_ref.at[g], o_all, s, o_up, o_dn, o_recv)
-    wait_slot(o_all, other, o_up, o_recv)
-    send_both(o_all.at[other], o_all, other, o_up, o_dn, o_recv)
-
-    width = wp_ref.shape[2]
-    ptile = chunk
+            @pl.when(j == R - 2)
+            def _():
+                start_o()
+
+            project_step(j)
+    else:
+        start_o()
 
     def rope(x, cosine, sine):
         lane = lax.broadcasted_iota(jnp.int32, x.shape, 1)
@@ -275,8 +346,7 @@
     @pl.loop(0, rows // ptile)
     def _(b):
         at = pl.ds(pl.multiple_of(b * ptile, ptile), ptile)
-        weights = w_all[...].reshape(-1, width)
-        y = jnp.dot(nrm[at, :], weights, preferred_element_type=F32)
+        y = yacc[at, :]
         cosine = cos_ref[at, :]
         sine = sin_ref[at, :]
         kv[r, at, 0:128] = rope(y[:, 128:256], cosine, sine).astype(BF16)
@@ -334,17 +404,22 @@
 
     @pl.loop(0, R - 1)
     def _(j):
-        line_step(j, o_all, o_up, o_dn, o_recv)
+        k = r - 1 - j
 
         @pl.when(j < r)
         def _():
-            k = r - 1 - j
             kv_copy(k).wait_recv()
 
             @pl.when(has_up)
             def _():
                 kv_copy(k).start()
 
+        @pl.when(j > 0)
+        def _():
+            line_step(j - 1, o_all, o_up, o_dn, o_recv)
+
+        @pl.when(j < r)
+        def _():
             attend(k, False)
 
     @pl.when(has_dn)
@@ -375,9 +450,21 @@
     cat[:, 0:128] = (diff * inv * hg_ref[...] * HEAD_SCALE).astype(BF16)
 
     share = rows // members
-    o_rows = o_all.shape[0] * o_all.shape[1]
-    half = o_rows // HALVES
-    o_slots = o_all.shape[0] // HALVES
+    half = part.shape[2]
+    o_slots = o_all.shape[0] // CHUNKS
+    if R == CHUNKS:
+        table = [sorted(range(R), key=lambda c: abs(c - i)) for i in range(R)]
+    else:
+        table = [list(range(CHUNKS))] * R
+
+    def chunk_at(k):
+        if R != CHUNKS:
+            return k
+        total = 0
+        for i in range(R):
+            total = total + jnp.where(r == i, table[i][k], 0)
+        return total
+
     orders = ([t_bits[0], x_dim] + t_bits[1:], t_bits + [x_dim])
 
     def block(mask):
@@ -391,7 +478,7 @@
         return found
 
     plans = []
-    for h in range(HALVES):
+    for h in range(CHUNKS):
         order = orders[h % 2]
         stages = []
         base = 0
@@ -423,26 +510,36 @@
             at = block(mask)
             part[h, at, :] = part[h, at, :] + rbuf[h, base + n].astype(F32)
 
-    for h in range(HALVES):
-        @pl.loop(0, 4)
+    def out_product(h):
+        first = chunk_at(h) * o_slots
+
+        @pl.loop(0, 2)
         def _(b):
-            at = pl.ds(pl.multiple_of(b * (rows // 4), rows // 4), rows // 4)
-            columns = o_all[h * o_slots : (h + 1) * o_slots].reshape(half, -1)
+            at = pl.ds(pl.multiple_of(b * (rows // 2), rows // 2), rows // 2)
+            columns = o_all[pl.ds(first, o_slots)].reshape(half, -1)
             part[h, at, :] = lax.dot_general(
                 cat[at, :], columns, (((1,), (1,)), ((), ())), preferred_element_type=F32
             )
 
-        rs_start(h, 0)
-
     levels = len(plans[0])
-    for i in range(levels):
-        for h in range(HALVES):
-            rs_finish(h, i)
-            if i + 1 < levels:
-                rs_start(h, i + 1)
     mine = block([])
-    for h in range(HALVES):
-        out_ref[:, h * half : (h + 1) * half] = part[h, mine, :].astype(BF16)
+    if R != CHUNKS:
+        line_step(R - 2, o_all, o_up, o_dn, o_recv)
+    for n in range(CHUNKS + levels):
+        for h in range(CHUNKS):
+            i = n - 1 - h
+            if 0 <= i < levels:
+                rs_finish(h, i)
+                if i + 1 < levels:
+                    rs_start(h, i + 1)
+                else:
+                    at = pl.ds(pl.multiple_of(chunk_at(h) * half, half), half)
+                    out_ref[:, at] = part[h, mine, :].astype(BF16)
+        if n < CHUNKS:
+            if n == CHUNKS - 1 and R == CHUNKS:
+                line_step(R - 2, o_all, o_up, o_dn, o_recv)
+            out_product(n)
+            rs_start(n, 0)
 
     cross_copy(wp_ref, w_all, wx_send, w_recv).wait_send()
     cross_copy(op_ref, o_all, ox_send, o_recv).wait_send()
@@ -460,7 +557,7 @@
         def _(k):
             kv_copy(k).wait_send()
 
-    for h in range(HALVES):
+    for h in range(CHUNKS):
         for dim, masks, base in plans[h]:
             for n, mask in enumerate(masks):
                 rs_copy(h, dim, mask, base + n).wait_send()
@@ -495,42 +592,27 @@
     members = G * tp
     share = rows // members
 
-    def heads_first(w):
-        return w.reshape(depth, G, -1)
-
-    packed = jnp.concatenate(
-        [
-            heads_first(w)
-            for w in (query_one, query_two, key_one, key_two, value_weight, pool_weight)
-        ],
-        axis=2,
-    ).transpose(1, 0, 2)
-    out_packed = jnp.concatenate(
-        [out_attn.reshape(G, VALUE_DIM, cols), out_pool.reshape(G, GROUP_DIM, cols)], axis=1
-    ).transpose(0, 2, 1)
-
-    line = lax.axis_index("sp") // G
     half_dim = HEAD_DIM // 2
-    lane = jnp.arange(2 * HEAD_DIM, dtype=jnp.int32)
-    inverse = ROPE_BASE ** (-((lane % half_dim).astype(F32) * 2.0 / HEAD_DIM))
-    positions = line * rows + jnp.arange(rows, dtype=jnp.int32)
-    angles = positions.astype(F32)[:, None] * inverse[None, :]
-    cosine = jnp.cos(angles)
-    sine = jnp.where(lane % HEAD_DIM < half_dim, -1.0, 1.0)[None, :] * jnp.sin(angles)
-
-    width = packed.shape[2]
-    depth_out = out_packed.shape[2]
+    inverse = ROPE_BASE ** (-((np.arange(2 * HEAD_DIM) % half_dim) * 2.0 / HEAD_DIM))
+    freq = jnp.asarray(inverse.astype(np.float32).reshape(1, -1))
+    width = 4 * HEAD_DIM + VALUE_DIM + GROUP_DIM
+    depth_out = VALUE_DIM + GROUP_DIM
     total_cols = sp * cols
     vm = pl.BlockSpec(memory_space=pltpu.VMEM)
     dma = pltpu.SemaphoreType.DMA
     return pl.pallas_call(
         functools.partial(kernel, (G, R, tp)),
         out_shape=jax.ShapeDtypeStruct((share, total_cols), BF16),
-        in_specs=[vm] * 6 + [pl.BlockSpec(memory_space=pltpu.SMEM)] + [vm] * 3,
+        in_specs=[vm] * 11 + [pl.BlockSpec(memory_space=pltpu.SMEM)] + [vm] * 3,
         out_specs=vm,
         scratch_shapes=[
+            pltpu.VMEM((G, depth, width), BF16),
+            pltpu.VMEM((G, cols, depth_out), BF16),
+            pltpu.VMEM((rows, 2 * HEAD_DIM), F32),
+            pltpu.VMEM((rows, 2 * HEAD_DIM), F32),
+            pltpu.VMEM((rows, width), F32),
             pltpu.VMEM((G, tp, chunk, feats), BF16),
-            pltpu.VMEM((rows, tp * feats), BF16),
+            pltpu.VMEM((R, rows, G * depth), BF16),
             pltpu.VMEM((sp, depth, width), BF16),
             pltpu.VMEM((sp, cols, depth_out), BF16),
             pltpu.VMEM((R, rows, 256), BF16),
@@ -542,9 +624,9 @@
             pltpu.VMEM((TAIL, GROUP_DIM), BF16),
             pltpu.VMEM((TAIL, GROUP_DIM), BF16),
             pltpu.VMEM((rows, depth_out), BF16),
-            pltpu.VMEM((HALVES, rows, total_cols // HALVES), F32),
-            pltpu.VMEM((HALVES, rows, total_cols // HALVES), BF16),
-            pltpu.VMEM((HALVES, members - 1, share, total_cols // HALVES), BF16),
+            pltpu.VMEM((CHUNKS, rows, total_cols // CHUNKS), F32),
+            pltpu.VMEM((CHUNKS, rows, total_cols // CHUNKS), BF16),
+            pltpu.VMEM((CHUNKS, members - 1, share, total_cols // CHUNKS), BF16),
             dma((members - 1,)),
             dma((members - 1,)),
             dma((sp,)),
@@ -559,8 +641,8 @@
             dma((R,)),
             dma,
             dma,
-            dma((HALVES, members - 1)),
-            dma((HALVES, members - 1)),
+            dma((CHUNKS, members - 1)),
+            dma((CHUNKS, members - 1)),
         ],
         compiler_params=pltpu.CompilerParams(
             collective_id=0, has_side_effects=True, vmem_limit_bytes=58 * 1024 * 1024
@@ -568,10 +650,15 @@
     )(
         tokens,
         norm_gain.reshape(1, -1),
-        packed,
-        out_packed,
-        cosine,
-        sine,
+        query_one,
+        key_one,
+        query_two,
+        key_two,
+        value_weight,
+        pool_weight,
+        out_attn,
+        out_pool,
+        freq,
         lambda_head,
         head_gain.reshape(1, -1),
         group_weight,

time: 106 us -> 103 us (0.972)
  Pallas kernels: 92.8 us -> 101 us
  local copies, waits for them, and re-layouts: 9.61 us -> 1.67 us
  other arithmetic: 2.57 us -> 0 us
    pallas_call x1, Pallas kernels: 92.8 us -> 101 us  [body(): pl.pallas_call(functools.partial(kernel, (G, R, tp)), out_shape=jax.Shape...]
    unnamed x21 -> x1, local copies, waits for them, and re-layouts: 7.59 us -> 1.67 us
    mul x1 -> x0, other arithmetic: 1.81 us -> none  [body(): jnp.where(lane % HEAD_DIM < half_dim, -1.0, 1.0)[None, :] * jnp.sin(angles)]
    concatenate x1 -> x0, local copies, waits for them, and re-layouts: 1.07 us -> none  [body(): jnp.concatenate([heads_first(w) for w in (query_one, query_two, key_one,...]
where the time goes in v2:
time: 103 us
  Pallas kernels  101 us (98%)
  local copies, waits for them, and re-layouts  1.67 us (2%)
    pallas_call x1, Pallas kernels, body(): pl.pallas_call(functools.partial(kernel, (G, R, tp)), out_shape=jax.Shape...  101 us

profile of v2, /device:TPU:26, one launch (start us, length us, event | category | flops | bytes accessed | tf_op | source)
XLA Modules:
  0.0 102.8 jit_solution(12440613140197675482)
XLA Ops:
  0.0 101.1 %shard_map.145 = bf16[64,2048]{1,0:T(8,128)(2,1)} custom-call(bf16[256,512]{1,0:T(8,128)(2,1)} %tok_ref.1, f32[1,2048]{1,0:T(1,128)} %bitcast.3, bf16[256,128]{1,0:T(8,128)(2,1)} %q1_ref.1, bf16[256,128]{1,0:T(8,128)(2,1)} %k1_ref.1, bf16[256,128]{1,0:T(8,128)(2,1)} %q2_ref.1, bf16[256,128]{1,0:T(8,128)(2,1)} %k2_ref.1, bf16[256,256]{1,0:T(8,128)(2,1)} %v_ref.1, ...), custom_call_target="tpu_custom_call" | custom-call | tf_op jit(solution)/shard_map/pallas_call | solution.py:603
  101.1 1.7 %copy.17 = bf16[64,2048]{1,0:T(8,128)(2,1)} copy(bf16[64,2048]{1,0:T(8,128)(2,1)} %shard_map.145) | data formatting | bytes 524288

commit v3 on v2

--- a/solution.py
+++ b/solution.py
@@ -17,7 +17,8 @@
 HEAD_FLOOR = 0.001
 MASKED = -1e30
 TAIL = 16
-CHUNKS = 4
+CHUNKS = 8
+PARTS = 2
 MESH = pl.DeviceIdType.MESH
 BF16 = jnp.bfloat16
 F32 = jnp.float32
@@ -452,18 +453,16 @@
     share = rows // members
     half = part.shape[2]
     o_slots = o_all.shape[0] // CHUNKS
-    if R == CHUNKS:
-        table = [sorted(range(R), key=lambda c: abs(c - i)) for i in range(R)]
-    else:
-        table = [list(range(CHUNKS))] * R
+    by_line = R * PARTS == CHUNKS
+    table = [sorted(range(R), key=lambda c: abs(c - i)) for i in range(R)]
 
     def chunk_at(k):
-        if R != CHUNKS:
+        if not by_line:
             return k
         total = 0
         for i in range(R):
-            total = total + jnp.where(r == i, table[i][k], 0)
-        return total
+            total = total + jnp.where(r == i, table[i][k // PARTS], 0)
+        return total * PARTS + k % PARTS
 
     orders = ([t_bits[0], x_dim] + t_bits[1:], t_bits + [x_dim])
 
@@ -523,23 +522,25 @@
 
     levels = len(plans[0])
     mine = block([])
-    if R != CHUNKS:
-        line_step(R - 2, o_all, o_up, o_dn, o_recv)
-    for n in range(CHUNKS + levels):
-        for h in range(CHUNKS):
-            i = n - 1 - h
-            if 0 <= i < levels:
+    last = lambda: line_step(R - 2, o_all, o_up, o_dn, o_recv)
+    if by_line:
+        batches = [range(CHUNKS - PARTS), range(CHUNKS - PARTS, CHUNKS)]
+    else:
+        batches = [range(CHUNKS)]
+    for n, batch in enumerate(batches):
+        if n == len(batches) - 1:
+            last()
+        for h in batch:
+            out_product(h)
+            rs_start(h, 0)
+        for i in range(levels):
+            for h in batch:
                 rs_finish(h, i)
                 if i + 1 < levels:
                     rs_start(h, i + 1)
                 else:
                     at = pl.ds(pl.multiple_of(chunk_at(h) * half, half), half)
                     out_ref[:, at] = part[h, mine, :].astype(BF16)
-        if n < CHUNKS:
-            if n == CHUNKS - 1 and R == CHUNKS:
-                line_step(R - 2, o_all, o_up, o_dn, o_recv)
-            out_product(n)
-            rs_start(n, 0)
 
     cross_copy(wp_ref, w_all, wx_send, w_recv).wait_send()
     cross_copy(op_ref, o_all, ox_send, o_recv).wait_send()

time: 103 us -> 97.5 us (0.947)
  Pallas kernels: 101 us -> 95.7 us
    pallas_call x1, Pallas kernels: 101 us -> 95.7 us  [body(): pl.pallas_call(functools.partial(kernel, (G, R, tp)), out_shape=jax.Shape...]
where the time goes in v3:
time: 97.5 us; the launch traced here: 97.4 us
  Pallas kernels  95.7 us (98%)
  local copies, waits for them, and re-layouts  1.67 us (2%)
    pallas_call x1, Pallas kernels, body(): pl.pallas_call(functools.partial(kernel, (G, R, tp)), out_shape=jax.Shape...  95.7 us

profile of v3, /device:TPU:26, one launch (start us, length us, event | category | flops | bytes accessed | tf_op | source)
XLA Modules:
  0.0 97.4 jit_solution(12665906525916452565)
XLA Ops:
  0.0 95.7 %shard_map.145 = bf16[64,2048]{1,0:T(8,128)(2,1)} custom-call(bf16[256,512]{1,0:T(8,128)(2,1)} %tok_ref.1, f32[1,2048]{1,0:T(1,128)} %bitcast.3, bf16[256,128]{1,0:T(8,128)(2,1)} %q1_ref.1, bf16[256,128]{1,0:T(8,128)(2,1)} %k1_ref.1, bf16[256,128]{1,0:T(8,128)(2,1)} %q2_ref.1, bf16[256,128]{1,0:T(8,128)(2,1)} %k2_ref.1, bf16[256,256]{1,0:T(8,128)(2,1)} %v_ref.1, ...), custom_call_target="tpu_custom_call" | custom-call | tf_op jit(solution)/shard_map/pallas_call | solution.py:604
  95.7 1.7 %copy.17 = bf16[64,2048]{1,0:T(8,128)(2,1)} copy(bf16[64,2048]{1,0:T(8,128)(2,1)} %shard_map.145) | data formatting | bytes 524288

commit v4 on v3

--- a/solution.py
+++ b/solution.py
@@ -527,20 +527,35 @@
         batches = [range(CHUNKS - PARTS), range(CHUNKS - PARTS, CHUNKS)]
     else:
         batches = [range(CHUNKS)]
-    for n, batch in enumerate(batches):
-        if n == len(batches) - 1:
-            last()
+    def begin(batch):
         for h in batch:
             out_product(h)
             rs_start(h, 0)
+
+    def advance(batch, i):
+        for h in batch:
+            rs_finish(h, i)
+            if i + 1 < levels:
+                rs_start(h, i + 1)
+            else:
+                at = pl.ds(pl.multiple_of(chunk_at(h) * half, half), half)
+                out_ref[:, at] = part[h, mine, :].astype(BF16)
+
+    if by_line:
+        early, late = batches
+        begin(early)
+        advance(early, 0)
+        last()
+        begin(late)
+        for i in range(1, levels):
+            advance(early, i)
+            advance(late, i - 1)
+        advance(late, levels - 1)
+    else:
+        last()
+        begin(batches[0])
         for i in range(levels):
-            for h in batch:
-                rs_finish(h, i)
-                if i + 1 < levels:
-                    rs_start(h, i + 1)
-                else:
-                    at = pl.ds(pl.multiple_of(chunk_at(h) * half, half), half)
-                    out_ref[:, at] = part[h, mine, :].astype(BF16)
+            advance(batches[0], i)
 
     cross_copy(wp_ref, w_all, wx_send, w_recv).wait_send()
     cross_copy(op_ref, o_all, ox_send, o_recv).wait_send()

time: 97.5 us -> 94.2 us (0.966); the launches traced: 97.4 us -> 93 us
  Pallas kernels: 95.7 us -> 91.3 us
    pallas_call x1, Pallas kernels: 95.7 us -> 91.3 us  [body(): pl.pallas_call(functools.partial(kernel, (G, R, tp)), out_shape=jax.Shape...]
where the time goes in v4:
time: 94.2 us; the launch traced here: 93 us
  Pallas kernels  91.3 us (97%)
  local copies, waits for them, and re-layouts  1.67 us (2%)
    pallas_call x1, Pallas kernels, body(): pl.pallas_call(functools.partial(kernel, (G, R, tp)), out_shape=jax.Shape...  91.3 us

profile of v4, /device:TPU:26, one launch (start us, length us, event | category | flops | bytes accessed | tf_op | source)
XLA Modules:
  0.0 93.0 jit_solution(14039387853958541348)
XLA Ops:
  0.0 91.3 %shard_map.145 = bf16[64,2048]{1,0:T(8,128)(2,1)} custom-call(bf16[256,512]{1,0:T(8,128)(2,1)} %tok_ref.1, f32[1,2048]{1,0:T(1,128)} %bitcast.3, bf16[256,128]{1,0:T(8,128)(2,1)} %q1_ref.1, bf16[256,128]{1,0:T(8,128)(2,1)} %k1_ref.1, bf16[256,128]{1,0:T(8,128)(2,1)} %q2_ref.1, bf16[256,128]{1,0:T(8,128)(2,1)} %k2_ref.1, bf16[256,256]{1,0:T(8,128)(2,1)} %v_ref.1, ...), custom_call_target="tpu_custom_call" | custom-call | tf_op jit(solution)/shard_map/pallas_call | solution.py:619
  91.4 1.7 %copy.17 = bf16[64,2048]{1,0:T(8,128)(2,1)} copy(bf16[64,2048]{1,0:T(8,128)(2,1)} %shard_map.145) | data formatting | bytes 524288
